TPU v7x, 32 devices: a whole 2x2x4 slice. The times are simulated.
32 devices in a mesh: fs: 8 (over z, y), tp: 4 (over x, core).
Axes of the slice: x: 2, y: 2, z: 4, core: 2. Of those that a mesh axis runs over, the one named last changes fastest.
Arguments:
- tokens: bfloat16 [8192, 2048], P('fs', 'tp'), may hold values from -6 to 6
- mixer_gain: float32 [2048], replicated, may hold values from 0.1 to 1.9
- conv_taps: bfloat16 [3, 1024], replicated, may hold values from -3.5 to 3.5
- outer_weight: bfloat16 [2048, 1024], P('fs', 'tp'), may hold values from -0.125 to 0.125
- inner_weight: bfloat16 [2048, 1024], P('fs', 'tp'), may hold values from -0.125 to 0.125
- value_weight: bfloat16 [2048, 1024], P('fs', 'tp'), may hold values from -0.125 to 0.125
- merge_weight: bfloat16 [1024, 2048], P('tp', 'fs'), may hold values from -0.25 to 0.25
- merge_gain: float32 [2048], replicated, may hold values from 0.1 to 1.9
- channel_gain: float32 [2048], replicated, may hold values from 0.1 to 1.9
- gate_weight: bfloat16 [2048, 5632], P('fs', 'tp'), may hold values from -0.125 to 0.125
- up_weight: bfloat16 [2048, 5632], P('fs', 'tp'), may hold values from -0.125 to 0.125
- down_weight: bfloat16 [5632, 2048], P('tp', 'fs'), may hold values from -0.109375 to 0.109375
- output_gain: float32 [2048], replicated, may hold values from 0.1 to 1.9
Outputs:
- layer_out: bfloat16 [8192, 2048], P('fs', 'tp')
All inputs are finite; a program needn't handle non-finite values.
Results may differ from a plain program's by a relative error of at most 0.018.
Values may be sent and summed in bfloat16 or wider, within the bound.
A program may use at most 128 MiB of HBM per device.

v0:
```python
import jax
import jax.numpy as jnp
from jax import lax
from jax.sharding import PartitionSpec as P

HEAD_DIM = 128
EPS = 1e-06


def normalize(values):
    floats = values.astype(jnp.float32)
    return floats * lax.rsqrt(jnp.mean(floats * floats, axis=-1, keepdims=True) + EPS)


def rounded_term(partial_value):
    return lax.optimization_barrier(partial_value.astype(jnp.bfloat16)).astype(jnp.float32)


def finish_scatter(summed, residual, gain_row, squares):
    floats = summed.astype(jnp.float32)
    columns = floats.shape[1]
    factor = lax.rsqrt(squares / (columns * lax.axis_size("tp")) + EPS)
    own_gain = lax.dynamic_slice_in_dim(gain_row, lax.axis_index("tp") * columns, columns)
    return (residual.astype(jnp.float32) + floats * factor[:, None] * own_gain).astype(jnp.bfloat16)


def shards(
    tokens,
    mixer_gain,
    conv_taps,
    outer_weight,
    inner_weight,
    value_weight,
    merge_weight,
    merge_gain,
    channel_gain,
    gate_weight,
    up_weight,
    down_weight,
    output_gain,
):
    whole_tokens = lax.all_gather(tokens, "tp", axis=1, tiled=True)
    normed = (normalize(whole_tokens) * mixer_gain).astype(jnp.bfloat16)
    length = normed.shape[0]
    channels = outer_weight.shape[1]
    full_outer, full_inner, full_value = (
        lax.all_gather(outer_weight, "fs", axis=0, tiled=True),
        lax.all_gather(inner_weight, "fs", axis=0, tiled=True),
        lax.all_gather(value_weight, "fs", axis=0, tiled=True),
    )
    outer = jnp.dot(normed, full_outer, preferred_element_type=jnp.float32)
    inner = jnp.dot(normed, full_inner, preferred_element_type=jnp.float32)
    value = jnp.dot(normed, full_value, preferred_element_type=jnp.float32)
    own_taps = lax.dynamic_slice_in_dim(
        conv_taps, lax.axis_index("tp") * channels, channels, 1
    ).astype(jnp.float32)
    signal = inner * value
    padded = jnp.pad(signal, ((2, 0), (0, 0)))
    conv = (
        own_taps[0] * padded[:length]
        + own_taps[1] * padded[1 : length + 1]
        + own_taps[2] * padded[2:]
    )
    gated = (outer * conv).reshape(length, channels // HEAD_DIM, HEAD_DIM)
    mixed = normalize(gated).reshape(length, channels).astype(jnp.bfloat16)
    merged_part = jnp.dot(
        mixed,
        lax.all_gather(merge_weight, "fs", axis=1, tiled=True),
        preferred_element_type=jnp.float32,
    )
    merged = lax.psum(rounded_term(merged_part).astype(jnp.bfloat16), "tp")
    first_full = (whole_tokens.astype(jnp.float32) + normalize(merged) * merge_gain).astype(
        jnp.bfloat16
    )
    width = tokens.shape[1]
    first = lax.dynamic_slice_in_dim(first_full, lax.axis_index("tp") * width, width, 1)
    normed2 = (normalize(first_full) * channel_gain).astype(jnp.bfloat16)
    full_gate, full_up = (
        lax.all_gather(gate_weight, "fs", axis=0, tiled=True),
        lax.all_gather(up_weight, "fs", axis=0, tiled=True),
    )
    gate = jnp.dot(normed2, full_gate, preferred_element_type=jnp.float32)
    upward = jnp.dot(normed2, full_up, preferred_element_type=jnp.float32)
    hidden = (jax.nn.silu(gate) * upward).astype(jnp.bfloat16)
    down_part = jnp.dot(
        hidden,
        lax.all_gather(down_weight, "fs", axis=1, tiled=True),
        preferred_element_type=jnp.float32,
    )
    down = lax.psum_scatter(
        rounded_term(down_part).astype(jnp.bfloat16), "tp", scatter_dimension=1, tiled=True
    )
    down_float = down.astype(jnp.float32)
    down_squares = lax.psum(jnp.sum(down_float * down_float, axis=1), "tp")
    return finish_scatter(down, first, output_gain, down_squares)


def solution(mesh):
    return jax.shard_map(
        shards,
        mesh=mesh,
        in_specs=(
            P("fs", "tp"),
            P(),
            P(),
            P("fs", "tp"),
            P("fs", "tp"),
            P("fs", "tp"),
            P("tp", "fs"),
            P(),
            P(),
            P("fs", "tp"),
            P("fs", "tp"),
            P("tp", "fs"),
            P(),
        ),
        out_specs=P("fs", "tp"),
        check_vma=False,
    )
```

profile of v0, /device:TPU:0, one launch (start us, length us, event | category | flops | bytes accessed | tf_op | source)
XLA Modules:
  0.0 661.4 jit_solution(1043669761443059637)
XLA Ops:
  6.5 0.0 copy-start.2
  6.5 0.0 all-gather.9.cloned.1.call-start
  6.5 0.7 all-gather.9.cloned.1.call-update
  7.3 0.0 all-gather.13.cloned.1.call-start
  7.3 0.7 all-gather.13.cloned.1.call-update
  8.0 0.0 all-gather.15.cloned.1.call-start
  8.1 0.7 all-gather.15.cloned.1.call-update
  8.7 0.0 all-gather.11.cloned.1.call-start
  8.8 0.5 all-gather.11.cloned.1.call-update
  9.3 0.0 all-gather.17.cloned.1.call-start
  9.4 0.5 all-gather.17.cloned.1.call-update
  9.9 0.0 all-reduce.3.cloned.1.call-start
  10.0 0.7 dynamic-slice_convert_fusion
  10.7 35.5 %all-gather.9.cloned.1.call-done = bf16[1024,2048]{1,0:T(8,128)(2,1)} async-done(((bf16[1024,512]{1,0:T(8,128)(2,1)}), bf16[1024,2048]{1,0:T(8,128)(2,1)}) %all-gather.9.cloned.1.call-update) | async-done | bytes 4194320 | tf_op jit(solution)/shard_map/all_gather | solution.py:42
  46.1 3.1 fusion.5
  49.2 39.4 %all-gather.13.cloned.1.call-done = bf16[2048,256]{1,0:T(8,128)(2,1)} async-done(((bf16[256,256]{1,0:T(8,128)(2,1)}), bf16[2048,256]{1,0:T(8,128)(2,1)}) %all-gather.13.cloned.1.call-update) | async-done | bytes 1048592 | tf_op jit(solution)/shard_map/all_gather | solution.py:48
  88.5 0.0 copy-done.2
  88.5 4.0 fusion.22
  92.5 37.2 %all-gather.15.cloned.1.call-done = bf16[2048,256]{1,0:T(8,128)(2,1)} async-done(((bf16[256,256]{1,0:T(8,128)(2,1)}), bf16[2048,256]{1,0:T(8,128)(2,1)}) %all-gather.15.cloned.1.call-update) | async-done | bytes 1048592 | tf_op jit(solution)/shard_map/all_gather | solution.py:49
  129.7 4.0 convolution_multiply_fusion
  133.7 37.0 %all-gather.11.cloned.1.call-done = bf16[2048,256]{1,0:T(8,128)(2,1)} async-done(((bf16[256,256]{1,0:T(8,128)(2,1)}), bf16[2048,256]{1,0:T(8,128)(2,1)}) %all-gather.11.cloned.1.call-update) | async-done | bytes 1048592 | tf_op jit(solution)/shard_map/all_gather | solution.py:47
  170.7 4.4 bitcast_reduce_fusion
  175.1 0.1 fusion.20
  175.2 35.5 %all-gather.17.cloned.1.call-done = bf16[256,2048]{1,0:T(8,128)(2,1)} async-done(((bf16[256,256]{1,0:T(8,128)(2,1)}), bf16[256,2048]{1,0:T(8,128)(2,1)}) %all-gather.17.cloned.1.call-update) | async-done | bytes 1048592 | tf_op jit(solution)/shard_map/all_gather | solution.py:68
  210.7 4.6 convolution_convert_fusion.1
  215.3 0.0 copy-start.1
  215.3 0.0 all-reduce.3.cloned.1.call-update
  215.3 0.0 all-gather.19.cloned.1.call-start
  215.4 0.7 all-gather.19.cloned.1.call-update
  216.1 0.0 all-gather.21.cloned.1.call-start
  216.1 0.7 all-gather.21.cloned.1.call-update
  216.8 0.0 all-gather.23.cloned.1.call-start
  216.9 0.7 all-gather.23.cloned.1.call-update
  217.5 0.2 reduce-scatter.2.cloned.1.call-start
  217.8 82.2 %all-reduce.3.cloned.1.call-done = bf16[1024,2048]{1,0:T(8,128)(2,1)} async-done(((bf16[1024,2048]{1,0:T(8,128)(2,1)}), bf16[1024,2048]{1,0:T(8,128)(2,1)}) %all-reduce.3.cloned.1.call-update) | async-done | bytes 4194320 | tf_op jit(solution)/shard_map/psum | solution.py:71
  300.0 0.0 copy-start
  300.0 3.2 fusion
  303.2 0.0 copy-done.1
  303.2 0.2 copy-done
  303.4 0.0 copy-start.3
  303.4 5.3 fusion.2
  308.8 85.9 %all-gather.19.cloned.1.call-done = bf16[2048,1408]{1,0:T(8,128)(2,1)} async-done(((bf16[256,1408]{1,0:T(8,128)(2,1)}), bf16[2048,1408]{1,0:T(8,128)(2,1)}) %all-gather.19.cloned.1.call-update) | async-done | bytes 5767184 | tf_op jit(solution)/shard_map/all_gather | solution.py:79
  394.6 0.0 copy-done.3
  394.6 12.0 %fusion.14 = f32[1024,1408]{1,0:T(8,128)} fusion(bf16[2048,1408]{1,0:T(8,128)(2,1)} %all-gather.19.cloned.1.call-done, bf16[1024,2048]{1,0:T(8,128)(2,1)} %get-tuple-element.6, f32[2048]{0:T(1024)S(1)} %copy-done.3, f32[1024]{0:T(1024)S(1)} %add_rsqrt_fusion.2), kind=kOutput, calls=%fused_computation.27 | convolution fusion | flops 5913968640 | bytes 15740928 | tf_op jit(solution)/shard_map/dot_general | solution.py:82
  406.6 80.7 %all-gather.21.cloned.1.call-done = bf16[2048,1408]{1,0:T(8,128)(2,1)} async-done(((bf16[256,1408]{1,0:T(8,128)(2,1)}), bf16[2048,1408]{1,0:T(8,128)(2,1)}) %all-gather.21.cloned.1.call-update) | async-done | bytes 5767184 | tf_op jit(solution)/shard_map/all_gather | solution.py:80
  487.3 93.4 %all-gather.23.cloned.1.call-done = bf16[1408,2048]{1,0:T(8,128)(2,1)} async-done(((bf16[1408,256]{1,0:T(8,128)(2,1)}), bf16[1408,2048]{1,0:T(8,128)(2,1)}) %all-gather.23.cloned.1.call-update) | async-done | bytes 5767184 | tf_op jit(solution)/shard_map/all_gather | solution.py:87
  580.7 20.8 %convolution_convert_fusion = bf16[1024,2048]{1,0:T(8,128)(2,1)} fusion(bf16[1408,2048]{1,0:T(8,128)(2,1)} %all-gather.23.cloned.1.call-done, f32[1024,1408]{1,0:T(8,128)} %fusion.14, bf16[2048,1408]{1,0:T(8,128)(2,1)} %all-gather.21.cloned.1.call-done, bf16[1024,2048]{1,0:T(8,128)(2,1)} %get-tuple-element.6, f32[2048]{0:T(1024)S(1)} %copy-done.3, ...), kind=kOutput, calls=%fused_computation.17 | convolution fusion | flops 11830296576 | bytes 25702400 | tf_op jit(solution)/shard_map/dot_general | solution.py:85
  601.6 0.0 reduce-scatter.2.cloned.1.call-update
  601.6 0.8 dynamic_slice.11
  602.3 42.0 %reduce-scatter.2.cloned.1.call-done = bf16[1024,512]{1,0:T(8,128)(2,1)} async-done(((bf16[1024,2048]{1,0:T(8,128)(2,1)}), bf16[1024,512]{1,0:T(8,128)(2,1)}) %reduce-scatter.2.cloned.1.call-update) | async-done | bytes 1048592 | tf_op jit(solution)/shard_map/reduce_scatter | solution.py:90
  644.3 1.5 fusion.9
  645.8 5.8 psum.15
  651.6 3.0 fusion.12
  (6 shorter events, 0.0 us)
Async XLA Ops:
  6.5 82.0 %copy-start.2 = (f32[2048]{0:T(1024)S(1)}, f32[2048]{0:T(1024)}, u32[]{:S(2)}) copy-start(f32[2048]{0:T(1024)} %param.14) | copy-start | bytes 24580
  6.5 39.6 %all-gather.9.cloned.1.call-start = ((), (), s32[]{:S(2)}) async-start(), calls=%async_computation.1 | async-start | bytes 5242880 | tf_op jit(solution)/shard_map/all_gather | solution.py:42
  7.3 81.3 %all-gather.13.cloned.1.call-start = ((), (), s32[]{:S(2)}) async-start(), calls=%async_computation.3 | async-start | bytes 1179648 | tf_op jit(solution)/shard_map/all_gather | solution.py:48
  8.0 121.7 %all-gather.15.cloned.1.call-start = ((), (), s32[]{:S(2)}) async-start(), calls=%async_computation.4 | async-start | bytes 1179648 | tf_op jit(solution)/shard_map/all_gather | solution.py:49
  8.7 162.0 %all-gather.11.cloned.1.call-start = ((), (), s32[]{:S(2)}) async-start(), calls=%async_computation.2 | async-start | bytes 1179648 | tf_op jit(solution)/shard_map/all_gather | solution.py:47
  9.3 201.4 %all-gather.17.cloned.1.call-start = ((), (), s32[]{:S(2)}) async-start(), calls=%async_computation.5 | async-start | bytes 1179648 | tf_op jit(solution)/shard_map/all_gather | solution.py:68
  9.9 290.1 %all-reduce.3.cloned.1.call-start = ((), (), s32[]{:S(2)}) async-start(), calls=%async_computation.6 | async-start | bytes 8388608 | tf_op jit(solution)/shard_map/psum | solution.py:71
  215.3 87.9 %copy-start.1 = (f32[2048]{0:T(1024)S(1)}, f32[2048]{0:T(1024)}, u32[]{:S(2)}) copy-start(f32[2048]{0:T(1024)} %param.20) | copy-start | bytes 24580
  215.3 179.3 %all-gather.19.cloned.1.call-start = ((), (), s32[]{:S(2)}) async-start(), calls=%async_computation.7 | async-start | bytes 6488064 | tf_op jit(solution)/shard_map/all_gather | solution.py:79
  216.1 271.3 %all-gather.21.cloned.1.call-start = ((), (), s32[]{:S(2)}) async-start(), calls=%async_computation.8 | async-start | bytes 6488064 | tf_op jit(solution)/shard_map/all_gather | solution.py:80
  216.8 363.9 %all-gather.23.cloned.1.call-start = ((), (), s32[]{:S(2)}) async-start(), calls=%async_computation.9 | async-start | bytes 6488064 | tf_op jit(solution)/shard_map/all_gather | solution.py:87
  217.5 426.8 %reduce-scatter.2.cloned.1.call-start = ((), (), s32[]{:S(2)}) async-start(), calls=%async_computation.10 | async-start | bytes 5242880 | tf_op jit(solution)/shard_map/reduce_scatter | solution.py:90
  300.0 3.4 copy-start
  303.4 91.2 %copy-start.3 = (f32[2048]{0:T(1024)S(1)}, f32[2048]{0:T(1024)}, u32[]{:S(2)}) copy-start(f32[2048]{0:T(1024)} %param.21) | copy-start | bytes 24580
Sparse Core Ops, SparseCore 0:
  8.9 37.1 all-gather.8
  48.2 40.2 all-gather.12
  90.7 38.9 all-gather.14
  131.7 38.9 all-gather.10
  172.6 38.0 all-gather.16
  215.4 84.4 all-reduce.2
  302.1 92.4 all-gather.18
  396.8 90.4 all-gather.20
  489.4 91.2 all-gather.22
  601.7 42.5 reduce-scatter.1
where the time goes:
time: 662 us; the launch traced here: 661 us
  waiting for transfers between devices  574 us (87%)
  matrix products  49.7 us (8%)
  other arithmetic  16.9 us (3%)
  between operations  13.6 us (2%)
    all_gather x1, waiting for transfers between devices, shards(): lax.all_gather(down_weight, 'fs', axis=1, tiled=True)  93.4 us
    all_gather x1, waiting for transfers between devices, shards(): lax.all_gather(gate_weight, 'fs', axis=0, tiled=True)  85.9 us
    psum x1, waiting for transfers between devices, shards(): merged = lax.psum(rounded_term(merged_part).astype(jnp.bfloat16), 'tp')  82.2 us
    all_gather x1, waiting for transfers between devices, shards(): lax.all_gather(up_weight, 'fs', axis=0, tiled=True)  80.7 us
    reduce_scatter x1, waiting for transfers between devices, shards(): lax.psum_scatter(rounded_term(down_part).astype(jnp.bfloat16), 'tp', scat...  42 us
    all_gather x1, waiting for transfers between devices, shards(): lax.all_gather(inner_weight, 'fs', axis=0, tiled=True)  39.4 us
    all_gather x1, waiting for transfers between devices, shards(): lax.all_gather(value_weight, 'fs', axis=0, tiled=True)  37.2 us
    all_gather x1, waiting for transfers between devices, shards(): lax.all_gather(outer_weight, 'fs', axis=0, tiled=True)  37 us
  transfers between devices with their start and end apart: 10, of which 10 were waited for; matrix products, arithmetic and copies ran while one was open for 6% of the time, Pallas kernels for 0%

commit v1 on v0

--- a/solution.py
+++ b/solution.py
@@ -5,6 +5,17 @@
 
 HEAD_DIM = 128
 EPS = 1e-06
+
+
+def around_the_ring(x, mesh_axis, dim):
+    size = lax.axis_size(mesh_axis)
+    forward = [(i, (i + 1) % size) for i in range(size)]
+    terms = [x]
+    for far in range(1, size):
+        terms = [lax.ppermute(terms[0], mesh_axis, forward), *terms]
+    full = jnp.concatenate(terms, axis=dim)
+    shift = (lax.axis_index(mesh_axis) + 1) * terms[-1].shape[dim]
+    return jnp.roll(full, shift, axis=dim)
 
 
 def normalize(values):
@@ -39,7 +50,7 @@
     down_weight,
     output_gain,
 ):
-    whole_tokens = lax.all_gather(tokens, "tp", axis=1, tiled=True)
+    whole_tokens = around_the_ring(tokens, "tp", 1)
     normed = (normalize(whole_tokens) * mixer_gain).astype(jnp.bfloat16)
     length = normed.shape[0]
     channels = outer_weight.shape[1]

time: 662 us -> 626 us (0.946)
  waiting for transfers between devices: 574 us -> 531 us
  local copies, waits for them, and re-layouts: 0.99 us -> 8.9 us
    ppermute x0 -> x3, waiting for transfers between devices: none -> 42.1 us  [around_the_ring(): terms = [lax.ppermute(terms[0], mesh_axis, forward), *terms]]
    all_gather x1, waiting for transfers between devices: 37.2 us -> 0.02 us  [shards(): lax.all_gather(value_weight, 'fs', axis=0, tiled=True)]
    all_gather x1 -> x0, waiting for transfers between devices: 35.5 us -> none  [shards(): whole_tokens = lax.all_gather(tokens, 'tp', axis=1, tiled=True)]
    all_gather x1, waiting for transfers between devices: 39.4 us -> 28.6 us  [shards(): lax.all_gather(inner_weight, 'fs', axis=0, tiled=True)]
    unnamed x8 -> x17, local copies, waits for them, and re-layouts: 0.21 us -> 7.98 us
  transfers between devices with their start and end apart: 10 -> 12, of which waited for: 10 -> 11; matrix products, arithmetic and copies ran while one was open for 6% -> 7% of each run, Pallas kernels for 0% -> 0%
where the time goes in v1:
time: 626 us; the launch traced here: 625 us
  waiting for transfers between devices  531 us (85%)
  matrix products  49.8 us (8%)
  other arithmetic  15.3 us (2%)
  between operations  13.4 us (2%)
  local copies, waits for them, and re-layouts  8.9 us (1%)
    all_gather x1, waiting for transfers between devices, shards(): lax.all_gather(down_weight, 'fs', axis=1, tiled=True)  93.4 us
    all_gather x1, waiting for transfers between devices, shards(): lax.all_gather(gate_weight, 'fs', axis=0, tiled=True)  85.4 us
    psum x1, waiting for transfers between devices, shards(): merged = lax.psum(rounded_term(merged_part).astype(jnp.bfloat16), 'tp')  82.3 us
    all_gather x1, waiting for transfers between devices, shards(): lax.all_gather(up_weight, 'fs', axis=0, tiled=True)  80.7 us
    ppermute x3, waiting for transfers between devices, around_the_ring(): terms = [lax.ppermute(terms[0], mesh_axis, forward), *terms]  42.1 us
    reduce_scatter x1, waiting for transfers between devices, shards(): lax.psum_scatter(rounded_term(down_part).astype(jnp.bfloat16), 'tp', scat...  42 us
    all_gather x1, waiting for transfers between devices, shards(): lax.all_gather(outer_weight, 'fs', axis=0, tiled=True)  37.1 us
    all_gather x1, waiting for transfers between devices, shards(): lax.all_gather(merge_weight, 'fs', axis=1, tiled=True)  35.5 us
  transfers between devices with their start and end apart: 12, of which 11 were waited for; matrix products, arithmetic and copies ran while one was open for 7% of the time, Pallas kernels for 0%

profile of v1, /device:TPU:0, one launch (start us, length us, event | category | flops | bytes accessed | tf_op | source)
XLA Modules:
  0.0 625.1 jit_solution(16301622205248985992)
XLA Ops:
  6.5 0.0 all-gather.12.cloned.1.call-start
  6.5 0.7 all-gather.12.cloned.1.call-update
  7.3 0.0 all-gather.10.cloned.1.call-start
  7.3 0.7 all-gather.10.cloned.1.call-update
  8.0 0.0 all-gather.8.cloned.1.call-start
  8.1 0.5 collective-permute-start
  8.6 0.1 all-gather.8.cloned.1.call-update
  8.7 0.0 all-gather.14.cloned.1.call-start
  8.8 14.4 %collective-permute-done = bf16[1024,512]{1,0:T(8,128)(2,1)S(1)} collective-permute-done((bf16[1024,512]{1,0:T(8,128)(2,1)}, bf16[1024,512]{1,0:T(8,128)(2,1)S(1)}, u32[]{:S(2)}, u32[]{:S(2)}) %collective-permute-start) | collective-permute-done | bytes 1048608 | tf_op jit(solution)/shard_map/ppermute | solution.py:15
  23.2 0.0 collective-permute-start.1
  23.2 14.2 %collective-permute-done.1 = bf16[1024,512]{1,0:T(8,128)(2,1)S(1)} collective-permute-done((bf16[1024,512]{1,0:T(8,128)(2,1)S(1)}, bf16[1024,512]{1,0:T(8,128)(2,1)S(1)}, u32[]{:S(2)}, u32[]{:S(2)}) %collective-permute-start.1) | collective-permute-done | bytes 1048608 | tf_op jit(solution)/shard_map/ppermute | solution.py:15
  37.4 0.0 collective-permute-start.2
  37.4 0.0 all-gather.14.cloned.1.call-update
  37.5 0.0 all-reduce.3.cloned.1.call-start
  37.5 0.7 dynamic-slice_convert_fusion
  38.2 13.5 %collective-permute-done.2 = bf16[1024,512]{1,0:T(8,128)(2,1)} collective-permute-done((bf16[1024,512]{1,0:T(8,128)(2,1)S(1)}, bf16[1024,512]{1,0:T(8,128)(2,1)}, u32[]{:S(2)}, u32[]{:S(2)}) %collective-permute-start.2) | collective-permute-done | bytes 1048608 | tf_op jit(solution)/shard_map/ppermute | solution.py:15
  51.8 1.4 constant_dynamic-update-slice_fusion.7
  53.1 0.2 constant_dynamic-update-slice_fusion.6
  53.3 0.0 copy-start.3
  53.3 0.1 constant_dynamic-update-slice_fusion.5
  53.5 1.4 constant_dynamic-update-slice_fusion.4
  54.9 1.4 constant_dynamic-update-slice_fusion.3
  56.2 0.2 constant_dynamic-update-slice_fusion.2
  56.4 0.2 constant_dynamic-update-slice_fusion.1
  56.6 0.0 copy-done.1
  56.6 0.1 constant_dynamic-update-slice_fusion
  56.7 3.2 copy-done
  60.0 0.9 fusion.5
  60.9 0.0 all-gather.12.cloned.1.call-done
  60.9 0.0 copy-done.3
  60.9 4.1 fusion.21
  65.0 28.6 %all-gather.10.cloned.1.call-done = bf16[2048,256]{1,0:T(8,128)(2,1)} async-done(((bf16[256,256]{1,0:T(8,128)(2,1)}), bf16[2048,256]{1,0:T(8,128)(2,1)}) %all-gather.10.cloned.1.call-update) | async-done | bytes 1048592 | tf_op jit(solution)/shard_map/all_gather | solution.py:59
  93.6 4.0 convolution_multiply_fusion
  97.6 37.1 %all-gather.8.cloned.1.call-done = bf16[2048,256]{1,0:T(8,128)(2,1)} async-done(((bf16[256,256]{1,0:T(8,128)(2,1)}), bf16[2048,256]{1,0:T(8,128)(2,1)}) %all-gather.8.cloned.1.call-update) | async-done | bytes 1048592 | tf_op jit(solution)/shard_map/all_gather | solution.py:58
  134.8 4.4 bitcast_reduce_fusion
  139.1 0.1 fusion.20
  139.2 0.0 copy-start.2
  139.3 35.5 %all-gather.14.cloned.1.call-done = bf16[256,2048]{1,0:T(8,128)(2,1)} async-done(((bf16[256,256]{1,0:T(8,128)(2,1)}), bf16[256,2048]{1,0:T(8,128)(2,1)}) %all-gather.14.cloned.1.call-update) | async-done | bytes 1048592 | tf_op jit(solution)/shard_map/all_gather | solution.py:79
  174.8 4.6 convolution_convert_fusion.1
  179.4 0.0 all-reduce.3.cloned.1.call-update
  179.4 0.0 all-gather.16.cloned.1.call-start
  179.4 0.5 all-gather.16.cloned.1.call-update
  180.0 0.0 all-gather.18.cloned.1.call-start
  180.0 0.7 all-gather.18.cloned.1.call-update
  180.7 0.0 all-gather.20.cloned.1.call-start
  180.8 0.7 all-gather.20.cloned.1.call-update
  181.5 0.0 copy-start.4
  181.5 0.2 reduce-scatter.2.cloned.1.call-start
  181.7 82.3 %all-reduce.3.cloned.1.call-done = bf16[1024,2048]{1,0:T(8,128)(2,1)} async-done(((bf16[1024,2048]{1,0:T(8,128)(2,1)}), bf16[1024,2048]{1,0:T(8,128)(2,1)}) %all-reduce.3.cloned.1.call-update) | async-done | bytes 4194320 | tf_op jit(solution)/shard_map/psum | solution.py:82
  264.0 3.1 fusion
  267.1 0.0 copy-done.2
  267.1 6.0 fusion.2
  273.2 85.4 %all-gather.16.cloned.1.call-done = bf16[2048,1408]{1,0:T(8,128)(2,1)} async-done(((bf16[256,1408]{1,0:T(8,128)(2,1)}), bf16[2048,1408]{1,0:T(8,128)(2,1)}) %all-gather.16.cloned.1.call-update) | async-done | bytes 5767184 | tf_op jit(solution)/shard_map/all_gather | solution.py:90
  358.6 0.0 copy-done.4
  358.6 12.0 %fusion.14 = f32[1024,1408]{1,0:T(8,128)} fusion(bf16[2048,1408]{1,0:T(8,128)(2,1)} %all-gather.16.cloned.1.call-done, bf16[1024,2048]{1,0:T(8,128)(2,1)} %get-tuple-element.6, f32[2048]{0:T(1024)S(1)} %copy-done.4, f32[1024]{0:T(1024)S(1)} %add_rsqrt_fusion.2), kind=kOutput, calls=%fused_computation.27 | convolution fusion | flops 5913968640 | bytes 15740928 | tf_op jit(solution)/shard_map/dot_general | solution.py:93
  370.5 80.7 %all-gather.18.cloned.1.call-done = bf16[2048,1408]{1,0:T(8,128)(2,1)} async-done(((bf16[256,1408]{1,0:T(8,128)(2,1)}), bf16[2048,1408]{1,0:T(8,128)(2,1)}) %all-gather.18.cloned.1.call-update) | async-done | bytes 5767184 | tf_op jit(solution)/shard_map/all_gather | solution.py:91
  451.3 93.4 %all-gather.20.cloned.1.call-done = bf16[1408,2048]{1,0:T(8,128)(2,1)} async-done(((bf16[1408,256]{1,0:T(8,128)(2,1)}), bf16[1408,2048]{1,0:T(8,128)(2,1)}) %all-gather.20.cloned.1.call-update) | async-done | bytes 5767184 | tf_op jit(solution)/shard_map/all_gather | solution.py:98
  544.7 20.9 %convolution_convert_fusion = bf16[1024,2048]{1,0:T(8,128)(2,1)} fusion(bf16[1408,2048]{1,0:T(8,128)(2,1)} %all-gather.20.cloned.1.call-done, f32[1024,1408]{1,0:T(8,128)} %fusion.14, bf16[2048,1408]{1,0:T(8,128)(2,1)} %all-gather.18.cloned.1.call-done, bf16[1024,2048]{1,0:T(8,128)(2,1)} %get-tuple-element.6, f32[2048]{0:T(1024)S(1)} %copy-done.4, ...), kind=kOutput, calls=%fused_computation.17 | convolution fusion | flops 11830296576 | bytes 25702400 | tf_op jit(solution)/shard_map/dot_general | solution.py:96
  565.6 0.0 reduce-scatter.2.cloned.1.call-update
  565.6 0.8 dynamic_slice.16
  566.3 42.0 %reduce-scatter.2.cloned.1.call-done = bf16[1024,512]{1,0:T(8,128)(2,1)} async-done(((bf16[1024,2048]{1,0:T(8,128)(2,1)}), bf16[1024,512]{1,0:T(8,128)(2,1)}) %reduce-scatter.2.cloned.1.call-update) | async-done | bytes 1048592 | tf_op jit(solution)/shard_map/reduce_scatter | solution.py:101
  608.3 1.5 fusion.9
  609.8 5.8 psum.15
  615.6 3.0 fusion.12
  (8 shorter events, 0.1 us)
Async XLA Ops:
  6.5 50.0 %copy-start.1 = (bf16[1024,512]{1,0:T(8,128)(2,1)S(1)}, bf16[1024,512]{1,0:T(8,128)(2,1)}, u32[]{:S(2)}) copy-start(bf16[1024,512]{1,0:T(8,128)(2,1)} %param.13) | copy-start | bytes 3145732
  6.5 54.3 %all-gather.12.cloned.1.call-start = ((), (), s32[]{:S(2)}) async-start(), calls=%async_computation.3 | async-start | bytes 1179648 | tf_op jit(solution)/shard_map/all_gather | solution.py:60
  7.3 86.4 %all-gather.10.cloned.1.call-start = ((), (), s32[]{:S(2)}) async-start(), calls=%async_computation.2 | async-start | bytes 1179648 | tf_op jit(solution)/shard_map/all_gather | solution.py:59
  8.0 126.8 %all-gather.8.cloned.1.call-start = ((), (), s32[]{:S(2)}) async-start(), calls=%async_computation.1 | async-start | bytes 1179648 | tf_op jit(solution)/shard_map/all_gather | solution.py:58
  8.1 15.2 %collective-permute-start = (bf16[1024,512]{1,0:T(8,128)(2,1)}, bf16[1024,512]{1,0:T(8,128)(2,1)S(1)}, u32[]{:S(2)}, u32[]{:S(2)}) collective-permute-start(bf16[1024,512]{1,0:T(8,128)(2,1)} %param.13), channel_id=1, source_target_pairs={{0,1},{1,2},{2,3},{3,0},{4,5},{5,6},{6,7},{7,4},{8,9},{9,10},{10,1... | collective-permute-start | bytes 3145736 | tf_op jit(solution)/shard_map/ppermute | solution.py:15
  8.7 166.1 %all-gather.14.cloned.1.call-start = ((), (), s32[]{:S(2)}) async-start(), calls=%async_computation.4 | async-start | bytes 1179648 | tf_op jit(solution)/shard_map/all_gather | solution.py:79
  23.2 14.2 %collective-permute-start.1 = (bf16[1024,512]{1,0:T(8,128)(2,1)S(1)}, bf16[1024,512]{1,0:T(8,128)(2,1)S(1)}, u32[]{:S(2)}, u32[]{:S(2)}) collective-permute-start(bf16[1024,512]{1,0:T(8,128)(2,1)S(1)} %collective-permute-done), channel_id=1, source_target_pairs={{0,1},{1,2},{2,3},{3,0},{4,5},{5,6},{6,7},{7,4},{8,9},{9,10},{10,1... | collective-permute-start | bytes 3145736 | tf_op jit(solution)/shard_map/ppermute | solution.py:15
  37.4 14.3 %collective-permute-start.2 = (bf16[1024,512]{1,0:T(8,128)(2,1)S(1)}, bf16[1024,512]{1,0:T(8,128)(2,1)}, u32[]{:S(2)}, u32[]{:S(2)}) collective-permute-start(bf16[1024,512]{1,0:T(8,128)(2,1)S(1)} %collective-permute-done.1), channel_id=1, source_target_pairs={{0,1},{1,2},{2,3},{3,0},{4,5},{5,6},{6,7},{7,4},{8,9},{9,10},{10,1... | collective-permute-start | bytes 3145736 | tf_op jit(solution)/shard_map/ppermute | solution.py:15
  37.5 226.6 %all-reduce.3.cloned.1.call-start = ((), (), s32[]{:S(2)}) async-start(), calls=%async_computation.5 | async-start | bytes 8388608 | tf_op jit(solution)/shard_map/psum | solution.py:82
  53.3 7.6 %copy-start.3 = (f32[2048]{0:T(1024)S(1)}, f32[2048]{0:T(1024)}, u32[]{:S(2)}) copy-start(f32[2048]{0:T(1024)} %param.14) | copy-start | bytes 24580
  56.7 3.2 copy-start
  139.2 127.9 %copy-start.2 = (f32[2048]{0:T(1024)S(1)}, f32[2048]{0:T(1024)}, u32[]{:S(2)}) copy-start(f32[2048]{0:T(1024)} %param.20) | copy-start | bytes 24580
  179.4 179.2 %all-gather.16.cloned.1.call-start = ((), (), s32[]{:S(2)}) async-start(), calls=%async_computation.6 | async-start | bytes 6488064 | tf_op jit(solution)/shard_map/all_gather | solution.py:90
  180.0 271.3 %all-gather.18.cloned.1.call-start = ((), (), s32[]{:S(2)}) async-start(), calls=%async_computation.7 | async-start | bytes 6488064 | tf_op jit(solution)/shard_map/all_gather | solution.py:91
  180.7 363.9 %all-gather.20.cloned.1.call-start = ((), (), s32[]{:S(2)}) async-start(), calls=%async_computation.8 | async-start | bytes 6488064 | tf_op jit(solution)/shard_map/all_gather | solution.py:98
  181.5 177.1 %copy-start.4 = (f32[2048]{0:T(1024)S(1)}, f32[2048]{0:T(1024)}, u32[]{:S(2)}) copy-start(f32[2048]{0:T(1024)} %param.21) | copy-start | bytes 24580
  181.5 426.8 %reduce-scatter.2.cloned.1.call-start = ((), (), s32[]{:S(2)}) async-start(), calls=%async_computation.9 | async-start | bytes 5242880 | tf_op jit(solution)/shard_map/reduce_scatter | solution.py:101
Sparse Core Ops, SparseCore 0:
  9.5 42.9 all-gather.11
  54.6 38.9 all-gather.9
  95.7 38.9 all-gather.7
  136.7 38.0 all-gather.13
  179.5 84.4 all-reduce.2
  266.1 92.4 all-gather.15
  360.8 90.4 all-gather.17
  453.3 91.2 all-gather.19
  565.7 42.5 reduce-scatter.1
